TPU v7x, 32 devices: a whole 2x2x4 slice. The times are simulated.
32 devices in a mesh: sp: 8 (over z, x), tp: 4 (over y, core).
Axes of the slice: x: 2, y: 2, z: 4, core: 2. Of those that a mesh axis runs over, the one named last changes fastest.
Arguments:
- query_a: bfloat16 [1024, 2048], P('sp', 'tp'), may hold values from -6 to 6
- key_a: bfloat16 [1024, 2048], P('sp', 'tp'), may hold values from -6 to 6
- value_a: bfloat16 [1024, 4096], P('sp', 'tp'), may hold values from -6 to 6
- query_b: bfloat16 [1024, 2048], P('sp', 'tp'), may hold values from -6 to 6
- key_b: bfloat16 [1024, 2048], P('sp', 'tp'), may hold values from -6 to 6
- value_b: bfloat16 [1024, 2048], P('sp', 'tp'), may hold values from -6 to 6
- in_gate: float32 [2, 2, 16, 1024], P(None, None, 'tp', 'sp'), may hold values from -6 to 300
- forget_gate: float32 [2, 2, 16, 1024], P(None, None, 'tp', 'sp'), may hold values from 0 to 14.1
- head_gain_a: float32 [16, 256], P('tp'), may hold values from 0.1 to 1.9
- head_gain_b: float32 [16, 128], P('tp'), may hold values from 0.1 to 1.9
- out_weight_a: bfloat16 [4096, 2048], P('tp'), may hold values from -0.078125 to 0.078125
- out_weight_b: bfloat16 [2048, 2048], P('tp'), may hold values from -0.078125 to 0.078125
- residual: bfloat16 [2048, 1024], P('tp', 'sp'), may hold values from -40 to 40
- norm_gain: float32 [2048], P('tp'), may hold values from 0.1 to 1.9
- routes: int32 [1024, 2], P('sp'), may hold values from 0 to 7, all different within a row; in each aligned block of 128 rows (0 to 127, 128 to 255, ...) at most 64 rows name the same one
- route_weights: float32 [1024, 2], P('sp'), may hold values from 0.2 to 1
- expert_gate: bfloat16 [8, 2048, 4096], P('sp', None, 'tp'), may hold values from -0.125 to 0.125
- expert_up: bfloat16 [8, 2048, 4096], P('sp', None, 'tp'), may hold values from -0.125 to 0.125
- expert_down: bfloat16 [8, 4096, 2048], P('sp', 'tp'), may hold values from -0.09375 to 0.09375
Outputs:
- layer_output: bfloat16 [2048, 1024], P('tp', 'sp')
Inputs may be any that keep to these rules, and one draw needn't show every extreme that they name: `routes`: each row names 2 different experts. In each aligned block of 128 rows (the rows of one index of sp) no expert is named by more than 64 rows, a bound that some blocks reach.
All inputs are finite; a program needn't handle non-finite values.
Results may differ from a plain program's by a relative error of at most 0.012.
Values may be sent and summed in bfloat16 or wider, within the bound.
A program may use at most 128 MiB of HBM per device.

v0:
```python
import jax
import jax.numpy as jnp
from jax import lax
from jax.sharding import PartitionSpec as P

BLOCK = 128


EPSILON = 1e-06
LOG_FLOOR = -1e30
PRECISE = lax.Precision.HIGH


def carried_in(value, axis, join, neutral, backward):
    count, mine = (lax.axis_size(axis), lax.axis_index(axis))
    pieces = jax.tree.map(lambda part: lax.all_gather(part, axis), value)
    if backward:
        pieces = jax.tree.map(lambda part: part[::-1], pieces)
        mine = count - 1 - mine
    so_far = jax.tree.map(
        lambda part, zero: jnp.full_like(part, 0) + jnp.asarray(zero, part.dtype), value, neutral
    )

    def turn(position, so_far):
        longer = join(so_far, jax.tree.map(lambda part: part[position], pieces))
        return jax.tree.map(lambda new, old: jnp.where(position < mine, new, old), longer, so_far)

    return lax.fori_loop(0, count - 1, turn, so_far)


def heads_first(tensor, head_count):
    return tensor.reshape(tensor.shape[0], head_count, -1).transpose(1, 0, 2)


def block_pass(queries, keys_in, values_in, log_input, log_decay, start):
    head_count, length, width_k = queries.shape
    blocks = length // BLOCK
    q_scale = width_k ** (-0.5)
    lower_mask = jnp.tril(jnp.ones((BLOCK, BLOCK), dtype=bool))

    def to_blocks(tensor):
        return jnp.moveaxis(tensor.reshape(head_count, blocks, BLOCK, *tensor.shape[2:]), 1, 0)

    def block_step(carried_state, inputs_block):
        memory, normal, stabilizer = carried_state
        q_block, k_block, v_block, in_block, decay_block = inputs_block
        cumulative = jnp.cumsum(decay_block, axis=-1)
        running_log_decay = cumulative + stabilizer[:, None]
        log_weights = jnp.where(
            lower_mask,
            cumulative[:, :, None] - cumulative[:, None, :] + in_block[:, None, :],
            -jnp.inf,
        )
        row_peak = jnp.maximum(running_log_decay, jnp.max(log_weights, axis=-1))
        carried_weight = jnp.exp(running_log_decay - row_peak)
        products = (
            jnp.einsum("htd,hsd->hts", q_block, k_block, preferred_element_type=jnp.float32)
            * q_scale
        )
        scores = products * jnp.exp(log_weights - row_peak[:, :, None])
        q_float = q_block.astype(jnp.float32) * q_scale
        numerator = carried_weight[:, :, None] * jnp.einsum(
            "htd,hde->hte", q_float, memory, precision=PRECISE
        )
        numerator = numerator + jnp.einsum(
            "hts,hse->hte", scores.astype(jnp.bfloat16), v_block, preferred_element_type=jnp.float32
        )
        denominator = carried_weight * jnp.einsum(
            "htd,hd->ht", q_float, normal, precision=PRECISE
        ) + jnp.sum(scores, axis=-1)
        decay_total = cumulative[:, -1]
        tail_logs = decay_total[:, None] - cumulative + in_block
        new_stabilizer = jnp.maximum(decay_total + stabilizer, jnp.max(tail_logs, axis=-1))
        keep_scale = jnp.exp(decay_total + stabilizer - new_stabilizer)
        weighted_keys = (
            k_block.astype(jnp.float32) * jnp.exp(tail_logs - new_stabilizer[:, None])[:, :, None]
        )
        memory = keep_scale[:, None, None] * memory + jnp.einsum(
            "hsd,hse->hde", weighted_keys, v_block.astype(jnp.float32), precision=PRECISE
        )
        normal = keep_scale[:, None] * normal + jnp.sum(weighted_keys, axis=1)
        return ((memory, normal, new_stabilizer), (numerator, denominator, row_peak))

    blocked = tuple(
        (to_blocks(tensor) for tensor in (queries, keys_in, values_in, log_input, log_decay))
    )
    final_state, outputs = lax.scan(block_step, start, blocked)
    joined = [
        jnp.moveaxis(tensor, 0, 1).reshape(head_count, length, *tensor.shape[3:])
        for tensor in outputs
    ]
    return (final_state, joined[0], joined[1], joined[2])


def device_summary(view):
    queries, keys_in, values_in, log_input, log_decay = view
    cumulative = jnp.cumsum(log_decay, axis=-1)
    decay_total = cumulative[:, -1]
    tail_logs = decay_total[:, None] - cumulative + log_input
    stabilizer = jnp.max(tail_logs, axis=-1)
    weighted_keys = (
        keys_in.astype(jnp.float32) * jnp.exp(tail_logs - stabilizer[:, None])[:, :, None]
    )
    memory = jnp.einsum(
        "hsd,hse->hde", weighted_keys, values_in.astype(jnp.float32), precision=PRECISE
    )
    return (decay_total, memory, jnp.sum(weighted_keys, axis=1), stabilizer)


def merge_group(earlier, later):
    drop_early, memory_early, normal_early, top_early = earlier
    drop_late, memory_late, normal_late, top_late = later
    shifted = drop_late + top_early
    merged_top = jnp.maximum(shifted, top_late)
    scale_early = jnp.exp(shifted - merged_top)
    scale_late = jnp.exp(top_late - merged_top)
    memory = scale_early[:, None, None] * memory_early + scale_late[:, None, None] * memory_late
    normal = scale_early[:, None] * normal_early + scale_late[:, None] * normal_late
    return (drop_early + drop_late, memory, normal, merged_top)


def join_states(earlier, later):
    return merge_group(earlier[:4], later[:4]) + merge_group(earlier[4:], later[4:])


def pass_states(pieces, backward):
    identity = tuple(
        (
            jnp.full_like(piece, LOG_FLOOR) if position % 4 == 3 else jnp.zeros_like(piece)
            for position, piece in enumerate(pieces)
        )
    )
    if backward:
        return carried_in(pieces, "sp", join_states, identity, True)
    return carried_in(pieces, "sp", join_states, identity, False)


def normalize(numerator, denominator, row_peak):
    return numerator / jnp.maximum(jnp.abs(denominator), jnp.exp(-row_peak))[:, :, None]


def direction_outputs(views, backward):
    finished = []
    pieces = ()
    for view in views:
        pieces = pieces + device_summary(view)
    incoming = pass_states(pieces, backward)
    for number in range(2):
        outcome = block_pass(*views[number], incoming[4 * number + 1 : 4 * number + 4])
        finished.append(normalize(outcome[1], outcome[2], outcome[3]))
    return finished


def local(
    query_a,
    key_a,
    value_a,
    query_b,
    key_b,
    value_b,
    in_gate,
    forget_gate,
    head_gain_a,
    head_gain_b,
    out_weight_a,
    out_weight_b,
    residual,
    norm_gain,
    routes,
    route_weights,
    expert_gate,
    expert_up,
    expert_down,
):
    head_count = head_gain_a.shape[0]
    log_decay = jax.nn.log_sigmoid(forget_gate)
    groups = (
        (
            heads_first(query_a, head_count),
            heads_first(key_a, head_count),
            heads_first(value_a, head_count),
        ),
        (
            heads_first(query_b, head_count),
            heads_first(key_b, head_count),
            heads_first(value_b, head_count),
        ),
    )
    results = []
    for direction in range(2):
        views = []
        for group_index in range(2):
            tensors = groups[group_index] + (
                in_gate[direction, group_index],
                log_decay[direction, group_index],
            )
            if direction == 1:
                tensors = tuple((jnp.flip(tensor, 1) for tensor in tensors))
            views.append(tensors)
        results.append(direction_outputs(views, direction == 1))
    normed_heads = []
    for group_index, head_gain in enumerate((head_gain_a, head_gain_b)):
        both = results[0][group_index] + jnp.flip(results[1][group_index], 1)
        scaled = (
            both
            * lax.rsqrt(jnp.mean(both * both, axis=-1, keepdims=True) + EPSILON)
            * head_gain[:, None, :]
        )
        normed_heads.append(scaled.astype(jnp.bfloat16))
    heads_a, heads_b = normed_heads
    weights_a = out_weight_a.reshape(head_count, -1, out_weight_a.shape[1])
    weights_b = out_weight_b.reshape(head_count, -1, out_weight_b.shape[1])
    first_term = jnp.einsum("hse,hec->cs", heads_a, weights_a, preferred_element_type=jnp.float32)
    mix = lax.psum_scatter(
        (
            first_term
            + jnp.einsum("hse,hec->cs", heads_b, weights_b, preferred_element_type=jnp.float32)
        ).astype(jnp.bfloat16),
        "tp",
        scatter_dimension=0,
        tiled=True,
    ).astype(jnp.float32)
    updated = residual.astype(jnp.float32) + mix
    squares = lax.psum(jnp.sum(updated * updated, axis=0), "tp")
    whole_width = residual.shape[0] * lax.axis_size("tp")
    normed = (
        updated * lax.rsqrt(squares / whole_width + EPSILON)[None, :] * norm_gain[:, None]
    ).astype(jnp.bfloat16)
    token_count = routes.shape[0]
    top_count = routes.shape[1]
    expert_count = lax.axis_size("sp") * expert_gate.shape[0]
    slot_count = 2 * token_count * top_count // expert_count
    flat_routes = routes.reshape(-1)
    hits = (flat_routes[:, None] == jnp.arange(expert_count, dtype=jnp.int32)[None, :]).astype(
        jnp.int32
    )
    ranks = jnp.sum((jnp.cumsum(hits, axis=0) - 1) * hits, axis=1)
    targets = (flat_routes * slot_count + ranks).reshape(token_count, top_count)
    slot_ids = jnp.arange(expert_count * slot_count, dtype=jnp.int32)[:, None]
    selectors = [
        (slot_ids == targets[None, :, ordering_index]).astype(jnp.bfloat16)
        for ordering_index in range(top_count)
    ]
    dispatch = selectors[0]
    ordering_index = 1
    dispatch = dispatch + selectors[ordering_index]
    buffer = jnp.einsum("ps,ds->pd", dispatch, normed, preferred_element_type=jnp.float32)
    buffer = buffer.astype(jnp.bfloat16).reshape(expert_count, slot_count, -1)
    arrived = lax.all_to_all(buffer, "sp", split_axis=0, concat_axis=0, tiled=True)
    piece = lax.all_gather(arrived, "tp", axis=2, tiled=True)
    flat_rows = piece.reshape(-1, piece.shape[-1])
    gate_rows = expert_gate[0]
    up_rows = expert_up[0]
    gate = jnp.dot(flat_rows, gate_rows, preferred_element_type=jnp.float32)
    upward = jnp.dot(flat_rows, up_rows, preferred_element_type=jnp.float32)
    hidden = (
        (jax.nn.silu(gate) * upward)
        .astype(jnp.bfloat16)
        .reshape(arrived.shape[0], arrived.shape[1], -1)
    )
    sources = hidden.shape[0]
    hidden_rows = hidden.reshape(-1, hidden.shape[-1])
    columns = expert_down[0]
    summed = lax.psum_scatter(
        jnp.einsum("rf,fc->cr", hidden_rows, columns, preferred_element_type=jnp.float32).astype(
            jnp.bfloat16
        ),
        "tp",
        scatter_dimension=0,
        tiled=True,
    ).astype(jnp.float32)
    outgoing = summed.astype(jnp.bfloat16).reshape(summed.shape[0], sources, slot_count)
    returned = lax.all_to_all(outgoing, "sp", split_axis=1, concat_axis=1, tiled=True)
    returned = returned.reshape(returned.shape[0], -1)
    combined = updated
    for ordering_index in range(top_count):
        picked = jnp.dot(returned, selectors[ordering_index], preferred_element_type=jnp.float32)
        combined = combined + route_weights[:, ordering_index][None, :] * picked
    return combined.astype(jnp.bfloat16)


def solution(mesh):
    placed = (
        P("sp", "tp"),
        P("sp", "tp"),
        P("sp", "tp"),
        P("sp", "tp"),
        P("sp", "tp"),
        P("sp", "tp"),
        P(None, None, "tp", "sp"),
        P(None, None, "tp", "sp"),
        P("tp", None),
        P("tp", None),
        P("tp", None),
        P("tp", None),
        P("tp", "sp"),
        P("tp"),
        P("sp", None),
        P("sp", None),
        P("sp", None, "tp"),
        P("sp", None, "tp"),
        P("sp", "tp", None),
    )
    return jax.shard_map(
        local, mesh=mesh, in_specs=placed, out_specs=P("tp", "sp"), check_vma=False
    )
```

profile of v0, /device:TPU:0, one launch (start us, length us, event | category | flops | bytes accessed | tf_op | source)
XLA Modules:
  0.0 495.7 jit_solution(4652735712022758953)
XLA Ops:
  23.3 1.4 fusion.72
  24.7 1.4 fusion.70
  26.7 1.4 fusion.78
  28.1 1.6 fusion.76
  43.1 1.4 dynamic-update-slice.2
  46.2 24.2 %all-reduce.8 = (f32[32]{0:T(128)}, f32[32]{0:T(128)}, f32[32]{0:T(128)}, f32[32]{0:T(128)}, f32[32]{0:T(128)}, /*index=5*/f32[32]{0:T(128)}, f32[32]{0:T(128)}, f32[32]{0:T(128)}) all-reduce(f32[32]{0:T(128)} %dynamic-update-slice.4, f32[32]{0:T(128)} %dynamic-update-slice.5, ...), channel_id=10, replica_groups=mesh['sp'=8,'tp'=4] {'sp'}, use_global_device_ids=true, to_apply=%add.4 | all-reduce | flops 256 | bytes 2048
  75.6 27.6 %all-gather.18 = f32[8,4,128]{2,1,0:T(4,128)} all-gather(f32[1,4,128]{2,1,0:T(4,128)} %bitcast.399), channel_id=13, replica_groups=mesh['sp'=8,'tp'=4] {'sp'}, dimensions={0}, use_global_device_ids=true | all-gather | bytes 18432 | tf_op jit(solution)/shard_map/all_gather | solution.py:16
  109.6 28.0 %all-gather.19 = f32[8,4,128]{2,1,0:T(4,128)} all-gather(f32[1,4,128]{2,1,0:T(4,128)} %bitcast.397), channel_id=17, replica_groups=mesh['sp'=8,'tp'=4] {'sp'}, dimensions={0}, use_global_device_ids=true | all-gather | bytes 18432 | tf_op jit(solution)/shard_map/all_gather | solution.py:16
  139.0 1.7 copy.163
  140.6 2.9 rev.81
  143.5 1.4 reshape.481
  146.2 27.1 %all-gather.16 = f32[8,4,128]{2,1,0:T(4,128)} all-gather(f32[1,4,128]{2,1,0:T(4,128)} %bitcast.398), channel_id=5, replica_groups=mesh['sp'=8,'tp'=4] {'sp'}, dimensions={0}, use_global_device_ids=true | all-gather | bytes 18432 | tf_op jit(solution)/shard_map/all_gather | solution.py:16
  175.9 27.5 %all-gather.17 = f32[8,4,128]{2,1,0:T(4,128)} all-gather(f32[1,4,128]{2,1,0:T(4,128)} %bitcast.396), channel_id=9, replica_groups=mesh['sp'=8,'tp'=4] {'sp'}, dimensions={0}, use_global_device_ids=true | all-gather | bytes 18432 | tf_op jit(solution)/shard_map/all_gather | solution.py:16
  203.4 1.7 copy.172
  205.1 2.9 rev.83
  208.0 2.0 fusion.65
  209.9 3.1 rev.79
  213.1 4.6 rev.71
  217.7 58.3 %while.11 = (s32[]{:T(128)}, f32[4,128,256]{2,1,0:T(8,128)S(1)}, f32[4,128]{1,0:T(4,128)}, f32[4]{0:T(128)}, f32[4,128,128]{2,1,0:T(8,128)}, /*index=5*/f32[4,12...) while((s32[]{:T(128)}, f32[4,128,256]{2,1,0:T(8,128)S(1)}, ...), condition=%wide.region_17.18_spmd.clone, body=%wide.region_16.17_spmd.clone.sunk | while | flops 988220 | bytes 2372229 | solution.py:28
  224.2 1.9 fusion.181
  232.5 1.9 fusion.181
  239.5 1.4 fusion.180
  240.8 1.9 fusion.181
  249.1 1.9 fusion.181
  257.5 1.9 fusion.181
  265.8 1.9 fusion.181
  274.1 1.9 fusion.181
  281.5 2.6 rev.82
  284.2 52.5 %while.10 = (s32[]{:T(128)}, f32[4,128,256]{2,1,0:T(8,128)S(1)}, f32[4,128]{1,0:T(4,128)S(1)}, f32[4]{0:T(128)}, f32[4,128,128]{2,1,0:T(8,128)S(1)}, /*index=5*/...) while((s32[]{:T(128)}, f32[4,128,256]{2,1,0:T(8,128)S(1)}, ...), condition=%wide.region_7.8_spmd.clone, body=%wide.region_6.7_spmd.clone.sunk | while | flops 988220 | bytes 2372229 | solution.py:28
  289.3 1.4 fusion.177
  296.8 1.4 fusion.177
  304.3 1.4 fusion.177
  311.8 1.4 fusion.177
  319.3 1.4 fusion.177
  326.7 1.4 fusion.177
  334.2 1.4 fusion.177
  341.6 1.9 rev.84
  347.0 3.0 convolution_bitcast_fusion
  350.0 1.4 fusion.42
  353.1 17.4 %reduce-scatter.3.cloned.1.call-done = bf16[512,128]{0,1:T(8,128)(2,1)} async-done(((bf16[2048,128]{0,1:T(8,128)(2,1)}), bf16[512,128]{0,1:T(8,128)(2,1)}) %reduce-scatter.3.cloned.1.call-update) | async-done | bytes 131088 | tf_op jit(solution)/shard_map/reduce_scatter | solution.py:214
  371.6 5.8 %psum.7 = f32[128]{0:T(128)S(1)} all-reduce(f32[128]{0:T(128)S(1)} %multiply_reduce_fusion.1), channel_id=1, replica_groups=mesh['sp'=8,'tp'=4] {'tp'}, use_global_device_ids=true, to_apply=%region_31.32 | all-reduce | flops 128 | bytes 1024 | tf_op jit(solution)/shard_map/psum | solution.py:224
  378.6 19.8 %all_to_all.10 = bf16[8,64,512]{2,1,0:T(8,128)(2,1)} all-to-all(bf16[8,64,512]{2,1,0:T(8,128)(2,1)S(1)} %bitcast.376), channel_id=1, replica_groups=mesh['sp'=8,'tp'=4] {'sp'}, dimensions={0} | all-to-all | bytes 1048576 | tf_op jit(solution)/shard_map/all_to_all | solution.py:249
  398.7 20.6 %all-gather.26.cloned.1.call-done = bf16[8,64,2048]{2,1,0:T(8,128)(2,1)} async-done(((bf16[8,64,512]{2,1,0:T(8,128)(2,1)}), bf16[8,64,2048]{2,1,0:T(8,128)(2,1)}) %all-gather.26.cloned.1.call-update) | async-done | bytes 2097168 | tf_op jit(solution)/shard_map/all_gather | solution.py:250
  419.3 6.5 %fusion.32 = f32[512,1024]{1,0:T(8,128)} fusion(bf16[512,2048]{1,0:T(8,128)(2,1)} %bitcast.404, bf16[1,2048,1024]{2,1,0:T(8,128)(2,1)} %param.39), kind=kOutput, calls=%fused_computation.64 | convolution fusion | flops 2147483648 | bytes 8388608 | tf_op jit(solution)/shard_map/dot_general | solution.py:254
  425.8 10.5 %fusion.37 = bf16[2048,512]{0,1:T(8,128)(2,1)} fusion(bf16[1,1024,2048]{2,1,0:T(8,128)(2,1)} %param.41, f32[512,1024]{1,0:T(8,128)} %fusion.32, bf16[512,2048]{1,0:T(8,128)(2,1)} %bitcast.405, bf16[1,2048,1024]{2,1,0:T(8,128)(2,1)} %param.40), kind=kOutput, calls=%fused_computation.67 | convolution fusion | flops 4299161600 | bytes 14680064 | tf_op jit(solution)/shard_map/rf,fc->cr/dot_general | solution.py:265
  436.4 31.3 %reduce-scatter.5.cloned.1.call-done = bf16[512,512]{0,1:T(8,128)(2,1)} async-done(((bf16[2048,512]{0,1:T(8,128)(2,1)}), bf16[512,512]{0,1:T(8,128)(2,1)}) %reduce-scatter.5.cloned.1.call-update) | async-done | bytes 524304 | tf_op jit(solution)/shard_map/reduce_scatter | solution.py:264
  467.7 5.5 %all-to-all-start.1 = ((bf16[512,8,64]{0,2,1:T(8,128)(2,1)}), bf16[512,8,64]{0,2,1:T(8,128)(2,1)S(1)}, u32[]{:S(2)}, u32[]{:S(2)}) async-start(bf16[512,8,64]{0,2,1:T(8,128)(2,1)} %bitcast.391), calls=%async_computation.3 | async-start | bytes 1048576 | tf_op jit(solution)/shard_map/all_to_all | solution.py:273
  473.2 14.3 %all-to-all-done.1 = bf16[512,8,64]{0,2,1:T(8,128)(2,1)S(1)} async-done(((bf16[512,8,64]{0,2,1:T(8,128)(2,1)}), bf16[512,8,64]{0,2,1:T(8,128)(2,1)S(1)}, u32[]{:S(2)}, u32[]{:S(2)}) %all-to-all-start.1) | async-done | bytes 524320 | tf_op jit(solution)/shard_map/all_to_all | solution.py:273
  (322 shorter events, 154.2 us)
Async XLA Ops:
  6.5 343.4 %copy-start = (bf16[512,2048]{1,0:T(8,128)(2,1)S(1)}, bf16[512,2048]{1,0:T(8,128)(2,1)}, u32[]{:S(2)}) copy-start(bf16[512,2048]{1,0:T(8,128)(2,1)} %param.34) | copy-start | bytes 6291460
  6.5 7.4 %copy-start.11 = (bf16[128,1024]{1,0:T(8,128)(2,1)S(1)}, bf16[128,1024]{1,0:T(8,128)(2,1)}, u32[]{:S(2)}) copy-start(bf16[128,1024]{1,0:T(8,128)(2,1)} %param.25) | copy-start | bytes 786436
  6.5 7.8 %copy-start.2 = (bf16[128,512]{1,0:T(8,128)(2,1)S(1)}, bf16[128,512]{1,0:T(8,128)(2,1)}, u32[]{:S(2)}) copy-start(bf16[128,512]{1,0:T(8,128)(2,1)} %param.24) | copy-start | bytes 393220
  6.5 203.4 %all-gather.34.cloned.1.call-start = ((), (), s32[]{:S(2)}) async-start(), calls=%async_computation.10 | async-start | bytes 2359296 | tf_op jit(solution)/shard_map/all_gather | solution.py:16
  9.9 4.1 copy-start.38
  10.0 4.0 copy-start.27
  11.1 2.9 copy-start.19
  12.1 8.5 %copy-start.7 = (bf16[128,512]{1,0:T(8,128)(2,1)S(1)}, bf16[128,512]{1,0:T(8,128)(2,1)}, u32[]{:S(2)}) copy-start(bf16[128,512]{1,0:T(8,128)(2,1)} %param.27) | copy-start | bytes 393220
  12.1 8.5 %copy-start.17 = (bf16[128,512]{1,0:T(8,128)(2,1)S(1)}, bf16[128,512]{1,0:T(8,128)(2,1)}, u32[]{:S(2)}) copy-start(bf16[128,512]{1,0:T(8,128)(2,1)} %param.28) | copy-start | bytes 393220
  12.3 12.4 %copy-start.9 = (bf16[4,128,128]{2,1,0:T(8,128)(2,1)}, bf16[4,128,128]{2,1,0:T(8,128)(2,1)S(1)}, u32[]{:S(2)}) copy-start(bf16[4,128,128]{2,1,0:T(8,128)(2,1)S(1)} %rev.77) | copy-start | bytes 393220
  13.7 199.3 %all-gather.32.cloned.1.call-start = ((), (), s32[]{:S(2)}) async-start(), calls=%async_computation.9 | async-start | bytes 4718592 | tf_op jit(solution)/shard_map/all_gather | solution.py:16
  14.0 2.7 copy-start.29
  14.4 8.7 %copy-start.13 = (bf16[4,128,256]{2,1,0:T(8,128)(2,1)}, bf16[4,128,256]{2,1,0:T(8,128)(2,1)S(1)}, u32[]{:S(2)}) copy-start(bf16[4,128,256]{2,1,0:T(8,128)(2,1)S(1)} %rev.70) | copy-start | bytes 786436
  14.6 12.1 %copy-start.4 = (bf16[4,128,128]{2,1,0:T(8,128)(2,1)}, bf16[4,128,128]{2,1,0:T(8,128)(2,1)S(1)}, u32[]{:S(2)}) copy-start(bf16[4,128,128]{2,1,0:T(8,128)(2,1)S(1)} %rev.69) | copy-start | bytes 393220
  15.1 4.8 copy-start.39
  15.3 4.6 copy-start.46
  15.4 2.3 copy-start.32
  16.7 267.5 %all-gather.30.cloned.1.call-start = ((), (), s32[]{:S(2)}) async-start(), calls=%async_computation.8 | async-start | bytes 2359296 | tf_op jit(solution)/shard_map/all_gather | solution.py:16
  18.9 4.2 copy-start.40
  18.9 4.2 copy-start.41
  19.8 3.3 copy-start.47
  19.8 3.3 copy-start.48
  20.7 2.5 copy-start.33
  20.7 2.5 copy-start.34
  21.8 262.3 %all-gather.28.cloned.1.call-start = ((), (), s32[]{:S(2)}) async-start(), calls=%async_computation.7 | async-start | bytes 4718592 | tf_op jit(solution)/shard_map/all_gather | solution.py:16
  23.2 347.4 %reduce-scatter.3.cloned.1.call-start = ((), (), s32[]{:S(2)}) async-start(), calls=%async_computation.4 | async-start | bytes 655360 | tf_op jit(solution)/shard_map/reduce_scatter | solution.py:214
  276.0 5.2 %copy-start.14 = (bf16[4,128,256]{2,1,0:T(8,128)(2,1)S(1)}, bf16[4,128,256]{2,1,0:T(8,128)(2,1)}, u32[]{:S(2)}) copy-start(bf16[4,128,256]{2,1,0:T(8,128)(2,1)} %copy-done.13) | copy-start | bytes 786436
  279.9 4.3 copy-start.24
  284.2 52.5 %copy-start.36 = (f32[4,128]{1,0:T(4,128)S(1)}, f32[4,128]{1,0:T(4,128)}, u32[]{:S(2)}) copy-start(f32[4,128]{1,0:T(4,128)} %get-tuple-element.806) | copy-start | bytes 6148
  284.2 53.3 %copy-start.5 = (bf16[128,512]{0,1:T(8,128)(2,1)S(1)}, bf16[128,512]{0,1:T(8,128)(2,1)}, u32[]{:S(2)}) copy-start(bf16[128,512]{0,1:T(8,128)(2,1)} %copy.163) | copy-start | bytes 393220
  284.2 53.3 %copy-start.23 = (pred[128,128]{0,1:T(8,128)(4,1)S(1)}, pred[128,128]{0,1:T(8,128)(4,1)}, u32[]{:S(2)}) copy-start(pred[128,128]{0,1:T(8,128)(4,1)} %iota_compare_fusion.4) | copy-start | bytes 49156
  284.2 53.3 %copy-start.37 = (f32[4,128]{1,0:T(4,128)S(1)}, f32[4,128]{1,0:T(4,128)}, u32[]{:S(2)}) copy-start(f32[4,128]{1,0:T(4,128)} %get-tuple-element.911) | copy-start | bytes 6148
  336.7 2.5 copy-start.12
  336.7 2.5 copy-start.16
  337.7 2.0 copy-start.10
  337.7 2.0 copy-start.15
  339.6 4.8 copy-start.3
  339.6 4.8 copy-start.8
  339.7 5.6 %copy-start.25 = (f32[4,128]{1,0:T(4,128)S(1)}, f32[4,128]{1,0:T(4,128)}, u32[]{:S(2)}) copy-start(f32[4,128]{1,0:T(4,128)} %get-tuple-element.697) | copy-start | bytes 6148
  340.0 6.7 %copy-start.18 = (bf16[128,512]{1,0:T(8,128)(2,1)S(1)}, bf16[128,512]{1,0:T(8,128)(2,1)}, u32[]{:S(2)}) copy-start(bf16[128,512]{1,0:T(8,128)(2,1)} %param.28) | copy-start | bytes 393220
  341.6 5.3 %copy-start.22 = (f32[4,256]{1,0:T(4,128)S(1)}, f32[4,256]{1,0:T(4,128)}, u32[]{:S(2)}) copy-start(f32[4,256]{1,0:T(4,128)} %param.31) | copy-start | bytes 12292
  346.9 3.0 copy-start.43
  350.0 27.4 %copy-start.44 = (f32[512]{0:T(512)S(1)}, f32[512]{0:T(512)}, u32[]{:S(2)}) copy-start(f32[512]{0:T(512)} %param.36) | copy-start | bytes 6148
  351.4 68.0 %all-gather.26.cloned.1.call-start = ((), (), s32[]{:S(2)}) async-start(), calls=%async_computation.5 | async-start | bytes 2621440 | tf_op jit(solution)/shard_map/all_gather | solution.py:250
  398.5 69.2 %reduce-scatter.5.cloned.1.call-start = ((), (), s32[]{:S(2)}) async-start(), calls=%async_computation.6 | async-start | bytes 2621440 | tf_op jit(solution)/shard_map/reduce_scatter | solution.py:264
  436.4 36.9 %copy-start.49 = (f32[128,2]{0,1:T(2,128)S(1)}, f32[128,2]{0,1:T(2,128)}, u32[]{:S(2)}) copy-start(f32[128,2]{0,1:T(2,128)} %param.38) | copy-start | bytes 3076
  436.4 51.2 %copy-start.6 = (bf16[512,128]{0,1:T(8,128)(2,1)S(1)}, bf16[512,128]{0,1:T(8,128)(2,1)}, u32[]{:S(2)}) copy-start(bf16[512,128]{0,1:T(8,128)(2,1)} %reduce-scatter.3.cloned.1.call-done) | copy-start | bytes 393220
  467.7 19.8 %all-to-all-start.1 = ((bf16[512,8,64]{0,2,1:T(8,128)(2,1)}), bf16[512,8,64]{0,2,1:T(8,128)(2,1)S(1)}, u32[]{:S(2)}, u32[]{:S(2)}) async-start(bf16[512,8,64]{0,2,1:T(8,128)(2,1)} %bitcast.391), calls=%async_computation.3 | async-start | bytes 1048576 | tf_op jit(solution)/shard_map/all_to_all | solution.py:273
  (10 other events, 16.6 us)
Sparse Core Ops, SparseCore 0:
  13.9 52.1 all-gather.33
  68.2 71.7 all-gather.31
  142.2 48.0 all-gather.29
  192.3 71.3 all-gather.27
  351.5 19.0 reduce-scatter.2
  398.6 20.7 all-gather.25
  436.5 31.1 reduce-scatter.4
where the time goes:
time: 501 us; the launch traced here: 496 us
  blocking collectives  160 us (32%)
  other arithmetic  131 us (26%)
  waiting for transfers between devices  83.8 us (17%)
  local copies, waits for them, and re-layouts  63 us (13%)
  matrix products  36.8 us (7%)
  between operations  15 us (3%)
  starting transfers between devices  5.98 us (1%)
    all_gather x4, blocking collectives, carried_in(): pieces = jax.tree.map(lambda part: lax.all_gather(part, axis), value)  110 us
    select_n x70, other arithmetic, turn(): jnp.where(position < mine, new, old)  91.2 us
    reduce_scatter x1, waiting for transfers between devices, local(): lax.psum_scatter(jnp.einsum('rf,fc->cr', hidden_rows, columns, preferred_...  31.3 us
    unnamed x1, blocking collectives  24.2 us
    all_gather x1, waiting for transfers between devices, local(): piece = lax.all_gather(arrived, 'tp', axis=2, tiled=True)  20.6 us
    all_to_all x1, blocking collectives, local(): lax.all_to_all(buffer, 'sp', split_axis=0, concat_axis=0, tiled=True)  19.8 us
    unnamed x121, local copies, waits for them, and re-layouts  19.5 us
    exp x28, other arithmetic, merge_group(): scale_early = jnp.exp(shifted - merged_top)  19.3 us
  transfers between devices with their start and end apart: 8, of which 4 were waited for; matrix products, arithmetic and copies ran while one was open for 27% of the time, Pallas kernels for 0%

commit v1 on v0

v1 whole, which is shorter than its diff:
```python
import jax
import jax.numpy as jnp
from jax import lax
from jax.experimental import pallas as pl
from jax.experimental.pallas import tpu as pltpu
from jax.sharding import PartitionSpec as P

EPSILON = 1e-06
NOTHING = -1e30


def dot(left, right, contract):
    return lax.dot_general(
        left, right, (contract, ((), ())), preferred_element_type=jnp.float32
    )


def one_head(query, key, value, keys, values, inner_row, outer_row, column, peak, gain):
    length, width_k = query.shape
    scale = width_k ** (-0.5)
    rows = lax.broadcasted_iota(jnp.int32, (length, length), 0)
    lanes = lax.broadcasted_iota(jnp.int32, (length, length), 1)
    near = dot(query, key, ((1,), (1,))) * scale
    far = dot(query, keys, ((1,), (1,))) * scale
    far_scores = [far * outer_row[r] for r in range(2)]
    far_sums = [jnp.sum(scores, axis=1, keepdims=True) for scores in far_scores]
    far_values = dot(
        jnp.concatenate([scores.astype(jnp.bfloat16) for scores in far_scores], axis=0),
        values,
        ((1,), (0,)),
    )
    both = None
    for r in range(2):
        keep = lanes <= rows if r == 0 else lanes >= rows
        logs = jnp.where(keep, column[r] + inner_row[r], NOTHING)
        carried_log = column[r] + peak[r]
        top = jnp.maximum(carried_log, jnp.max(logs, axis=1, keepdims=True))
        carried = jnp.exp(carried_log - top)
        scores = near * jnp.exp(logs - top)
        numer = carried * far_values[r * length : (r + 1) * length] + dot(
            scores.astype(jnp.bfloat16), value, ((1,), (0,))
        )
        denom = carried * far_sums[r] + jnp.sum(scores, axis=1, keepdims=True)
        out = numer / jnp.maximum(jnp.abs(denom), jnp.exp(-top))
        both = out if both is None else both + out
    mean = jnp.mean(both * both, axis=1, keepdims=True)
    return (both * lax.rsqrt(mean + EPSILON) * gain).astype(jnp.bfloat16)


def mixer_kernel(
    qa, ka, va, qb, kb, vb, all_ka, all_va, all_kb, all_vb,
    inner, outer, column, peak, gain_a, gain_b, heads_a, heads_b,
):
    parts = (
        (qa, ka, va, all_ka, all_va, gain_a, heads_a),
        (qb, kb, vb, all_kb, all_vb, gain_b, heads_b),
    )
    for g, (q, k, v, every_k, every_v, gain, heads) in enumerate(parts):
        heads[...] = one_head(
            q[...], k[...], v[...], every_k[...], every_v[...],
            [inner[0, 2 * r + g : 2 * r + g + 1, :] for r in range(2)],
            [outer[0, 2 * r + g : 2 * r + g + 1, :] for r in range(2)],
            [column[0, :, 2 * r + g : 2 * r + g + 1] for r in range(2)],
            [peak[0, 2 * r + g : 2 * r + g + 1, 0:1] for r in range(2)],
            gain[0],
        )


def mix_heads(query_a, key_a, value_a, query_b, key_b, value_b, in_gate, forget_gate, gain_a, gain_b):
    heads = gain_a.shape[0]
    length = query_a.shape[0]
    width_k = query_a.shape[1] // heads
    width_a, width_b = gain_a.shape[1], gain_b.shape[1]
    count, mine = lax.axis_size("sp"), lax.axis_index("sp")
    packed = jnp.concatenate([value_a, key_a, key_b, value_b], axis=1)
    gathered = lax.all_gather(packed, "sp", axis=0, tiled=True)
    total_rows = gathered.shape[0]
    log_decay = jax.nn.log_sigmoid(forget_gate)
    ones = jnp.ones((length, length), jnp.float32)
    exact = lax.Precision.HIGHEST
    run = jnp.stack(
        [
            jnp.einsum("ghs,st->ght", log_decay[0], jnp.triu(ones), precision=exact),
            jnp.einsum("ghs,st->ght", log_decay[1], jnp.tril(ones), precision=exact),
        ]
    )
    whole = jnp.sum(log_decay, axis=-1, keepdims=True)
    tails = in_gate + whole - run
    small = lax.all_gather(
        jnp.stack([tails, jnp.broadcast_to(whole, tails.shape)]), "sp", axis=0
    )
    every_tail, every_whole = small[:, 0], small[:, 1, ..., 0]
    place = jnp.arange(count)
    source, middle = place[:, None], place[None, :]
    between = jnp.stack(
        [
            (middle > source) & (middle < mine),
            (middle < source) & (middle > mine),
        ]
    ).astype(jnp.float32)
    gap = jnp.sum(between[:, :, :, None, None] * jnp.moveaxis(every_whole, 0, 1)[:, None], axis=2)
    seen = jnp.stack([place < mine, place > mine])[:, :, None, None, None]
    logs = jnp.where(seen, jnp.moveaxis(every_tail, 0, 1) + gap[..., None], NOTHING)
    peak = jnp.max(logs, axis=(1, 4))
    outer = jnp.where(seen, jnp.exp(logs - peak[:, None, :, :, None]), 0.0)
    outer = outer.transpose(3, 0, 2, 1, 4).reshape(heads, 4, total_rows)
    peak = jnp.broadcast_to(peak.transpose(2, 0, 1).reshape(heads, 4, 1), (heads, 4, 128))
    inner = (in_gate - run).transpose(2, 0, 1, 3).reshape(heads, 4, length)
    column = run.transpose(2, 3, 0, 1).reshape(heads, length, 4)
    ratio = width_a // width_k

    def columns(rows, width, first):
        return pl.BlockSpec((rows, width), lambda h: (0, first + h))

    def by_head(*shape):
        return pl.BlockSpec((1,) + shape, lambda h: (h, 0, 0))

    return pl.pallas_call(
        mixer_kernel,
        grid=(heads,),
        in_specs=[
            columns(length, width_k, 0),
            columns(length, width_k, 0),
            columns(length, width_a, 0),
            columns(length, width_k, 0),
            columns(length, width_k, 0),
            columns(length, width_b, 0),
            columns(total_rows, width_k, ratio * heads),
            columns(total_rows, width_a, 0),
            columns(total_rows, width_k, (ratio + 1) * heads),
            columns(total_rows, width_b, (ratio + 2) * heads),
            by_head(4, length),
            by_head(4, total_rows),
            by_head(length, 4),
            by_head(4, 128),
            by_head(1, width_a),
            by_head(1, width_b),
        ],
        out_specs=[columns(length, width_a, 0), columns(length, width_b, 0)],
        out_shape=[
            jax.ShapeDtypeStruct((length, heads * width_a), jnp.bfloat16),
            jax.ShapeDtypeStruct((length, heads * width_b), jnp.bfloat16),
        ],
        cost_estimate=pl.CostEstimate(
            flops=4 * heads * length * total_rows * (2 * width_k + 2 * width_a),
            bytes_accessed=2 * packed.size * count,
            transcendentals=0,
        ),
    )(
        query_a, key_a, value_a, query_b, key_b, value_b,
        gathered, gathered, gathered, gathered,
        inner, outer, column, peak, gain_a[:, None, :], gain_b[:, None, :],
    )


def local(
    query_a,
    key_a,
    value_a,
    query_b,
    key_b,
    value_b,
    in_gate,
    forget_gate,
    head_gain_a,
    head_gain_b,
    out_weight_a,
    out_weight_b,
    residual,
    norm_gain,
    routes,
    route_weights,
    expert_gate,
    expert_up,
    expert_down,
):
    heads_a, heads_b = mix_heads(
        query_a, key_a, value_a, query_b, key_b, value_b,
        in_gate, forget_gate, head_gain_a, head_gain_b,
    )
    first_term = jnp.einsum("ec,se->cs", out_weight_a, heads_a, preferred_element_type=jnp.float32)
    mix = lax.psum_scatter(
        (
            first_term
            + jnp.einsum("ec,se->cs", out_weight_b, heads_b, preferred_element_type=jnp.float32)
        ).astype(jnp.bfloat16),
        "tp",
        scatter_dimension=0,
        tiled=True,
    ).astype(jnp.float32)
    updated = residual.astype(jnp.float32) + mix
    squares = lax.psum(jnp.sum(updated * updated, axis=0), "tp")
    whole_width = residual.shape[0] * lax.axis_size("tp")
    normed = (
        updated * lax.rsqrt(squares / whole_width + EPSILON)[None, :] * norm_gain[:, None]
    ).astype(jnp.bfloat16)
    token_count = routes.shape[0]
    top_count = routes.shape[1]
    expert_count = lax.axis_size("sp") * expert_gate.shape[0]
    slot_count = 2 * token_count * top_count // expert_count
    flat_routes = routes.reshape(-1)
    hits = (flat_routes[:, None] == jnp.arange(expert_count, dtype=jnp.int32)[None, :]).astype(
        jnp.int32
    )
    ranks = jnp.sum((jnp.cumsum(hits, axis=0) - 1) * hits, axis=1)
    targets = (flat_routes * slot_count + ranks).reshape(token_count, top_count)
    slot_ids = jnp.arange(expert_count * slot_count, dtype=jnp.int32)[:, None]
    selectors = [
        (slot_ids == targets[None, :, ordering_index]).astype(jnp.bfloat16)
        for ordering_index in range(top_count)
    ]
    dispatch = selectors[0]
    ordering_index = 1
    dispatch = dispatch + selectors[ordering_index]
    buffer = jnp.einsum("ps,ds->pd", dispatch, normed, preferred_element_type=jnp.float32)
    buffer = buffer.astype(jnp.bfloat16).reshape(expert_count, slot_count, -1)
    arrived = lax.all_to_all(buffer, "sp", split_axis=0, concat_axis=0, tiled=True)
    piece = lax.all_gather(arrived, "tp", axis=2, tiled=True)
    flat_rows = piece.reshape(-1, piece.shape[-1])
    gate_rows = expert_gate[0]
    up_rows = expert_up[0]
    gate = jnp.dot(flat_rows, gate_rows, preferred_element_type=jnp.float32)
    upward = jnp.dot(flat_rows, up_rows, preferred_element_type=jnp.float32)
    hidden = (
        (jax.nn.silu(gate) * upward)
        .astype(jnp.bfloat16)
        .reshape(arrived.shape[0], arrived.shape[1], -1)
    )
    sources = hidden.shape[0]
    hidden_rows = hidden.reshape(-1, hidden.shape[-1])
    columns = expert_down[0]
    summed = lax.psum_scatter(
        jnp.einsum("rf,fc->cr", hidden_rows, columns, preferred_element_type=jnp.float32).astype(
            jnp.bfloat16
        ),
        "tp",
        scatter_dimension=0,
        tiled=True,
    ).astype(jnp.float32)
    outgoing = summed.astype(jnp.bfloat16).reshape(summed.shape[0], sources, slot_count)
    returned = lax.all_to_all(outgoing, "sp", split_axis=1, concat_axis=1, tiled=True)
    returned = returned.reshape(returned.shape[0], -1)
    combined = updated
    for ordering_index in range(top_count):
        picked = jnp.dot(returned, selectors[ordering_index], preferred_element_type=jnp.float32)
        combined = combined + route_weights[:, ordering_index][None, :] * picked
    return combined.astype(jnp.bfloat16)


def solution(mesh):
    placed = (
        P("sp", "tp"),
        P("sp", "tp"),
        P("sp", "tp"),
        P("sp", "tp"),
        P("sp", "tp"),
        P("sp", "tp"),
        P(None, None, "tp", "sp"),
        P(None, None, "tp", "sp"),
        P("tp", None),
        P("tp", None),
        P("tp", None),
        P("tp", None),
        P("tp", "sp"),
        P("tp"),
        P("sp", None),
        P("sp", None),
        P("sp", None, "tp"),
        P("sp", None, "tp"),
        P("sp", "tp", None),
    )
    return jax.shard_map(
        local, mesh=mesh, in_specs=placed, out_specs=P("tp", "sp"), check_vma=False
    )
```

time: 501 us -> 257 us (0.51); the launches traced: 496 us -> 257 us
  other arithmetic: 131 us -> 5.3 us
  blocking collectives: 160 us -> 59 us
  local copies, waits for them, and re-layouts: 63 us -> 5.55 us
  waiting for transfers between devices: 83.8 us -> 136 us
  matrix products: 36.8 us -> 23.6 us
  Pallas kernels: 0 us -> 7.9 us
    select_n x70 -> x1, other arithmetic: 91.2 us -> 0.11 us  [mix_heads(): outer = jnp.where(seen, jnp.exp(logs - peak[:, None, :, :, None]), 0.0)]
    all_gather x4 -> x1, blocking collectives: 110 us -> 33.4 us  [mix_heads(): lax.all_gather(jnp.stack([tails, jnp.broadcast_to(whole, tails.shape)]),...]
    all_gather x4 -> x1, waiting for transfers between devices: 0.01 us -> 51.7 us  [mix_heads(): gathered = lax.all_gather(packed, 'sp', axis=0, tiled=True)]
    rev x20 -> x0, local copies, waits for them, and re-layouts: 27.1 us -> none  [the longest x8 15.5 us: carried_in(): pieces = jax.tree.map(lambda part: part[::-1], pieces)]
    unnamed x1 -> x0, blocking collectives: 24.2 us -> none
    exp x31 -> x0, other arithmetic: 20.2 us -> none  [the longest x28 19.3 us: merge_group(): scale_early = jnp.exp(shifted - merged_top)]
    unnamed x121 -> x21, local copies, waits for them, and re-layouts: 19.5 us -> 0.45 us
    dot_general x22 -> x4, matrix products: 17.9 us -> 4.73 us  [the longest x1 3.02 us: local(): jnp.einsum('ec,se->cs', out_weight_a, heads_a, preferred_element_type=jnp...]
  transfers between devices with their start and end apart: 8 -> 5, of which waited for: 4 -> 5; matrix products, arithmetic and copies ran while one was open for 27% -> 3% of each run, Pallas kernels for 0% -> 0%
where the time goes in v1:
time: 257 us
  waiting for transfers between devices  136 us (53%)
  blocking collectives  59 us (23%)
  matrix products  23.6 us (9%)
  between operations  13.4 us (5%)
  Pallas kernels  7.9 us (3%)
  starting transfers between devices  5.64 us (2%)
  local copies, waits for them, and re-layouts  5.55 us (2%)
  other arithmetic  5.3 us (2%)
    all_gather x1, waiting for transfers between devices, mix_heads(): gathered = lax.all_gather(packed, 'sp', axis=0, tiled=True)  51.7 us
    all_gather x1, blocking collectives, mix_heads(): lax.all_gather(jnp.stack([tails, jnp.broadcast_to(whole, tails.shape)]),...  33.4 us
    reduce_scatter x1, waiting for transfers between devices, local(): lax.psum_scatter(jnp.einsum('rf,fc->cr', hidden_rows, columns, preferred_...  31.3 us
    all_gather x1, waiting for transfers between devices, local(): piece = lax.all_gather(arrived, 'tp', axis=2, tiled=True)  20.8 us
    all_to_all x1, blocking collectives, local(): lax.all_to_all(buffer, 'sp', split_axis=0, concat_axis=0, tiled=True)  19.8 us
    reduce_scatter x1, waiting for transfers between devices, local(): lax.psum_scatter((first_term + jnp.einsum('ec,se->cs', out_weight_b, head...  18.2 us
    all_to_all x1, waiting for transfers between devices, local(): lax.all_to_all(outgoing, 'sp', split_axis=1, concat_axis=1, tiled=True)  14.3 us
    dot_general x1, matrix products, local(): jnp.einsum('rf,fc->cr', hidden_rows, columns, preferred_element_type=jnp....  10.5 us
  transfers between devices with their start and end apart: 5, of which 5 were waited for; matrix products, arithmetic and copies ran while one was open for 3% of the time, Pallas kernels for 0%

profile of v1, /device:TPU:0, one launch (start us, length us, event | category | flops | bytes accessed | tf_op | source)
XLA Modules:
  0.0 256.8 jit_solution(14884018941079509257)
XLA Ops:
  6.5 2.2 pad_maximum_fusion
  8.8 0.0 reduce-scatter.3.cloned.1.call-start
  8.8 0.8 fusion.56
  9.6 0.2 convolution_bitcast_fusion
  9.8 0.2 convolution_bitcast_fusion.1
  10.0 0.1 subtract_bitcast_fusion
  10.1 0.1 stack_broadcast_in_dim.2
  10.2 33.4 %all-gather = f32[16,2,2,4,128]{4,3,2,1,0:T(4,128)S(1)} all-gather(f32[2,2,2,4,128]{4,3,2,1,0:T(4,128)S(1)} %pad_maximum_fusion.1), channel_id=2, replica_groups=mesh['sp'=8,'tp'=4] {'sp'}, dimensions={0}, use_global_device_ids=true | all-gather | bytes 147456 | tf_op jit(solution)/shard_map/all_gather | solution.py:89
  43.7 0.2 copy.117
  43.9 0.1 multiply_reduce_fusion.1
  44.0 0.2 fusion.33
  44.2 0.1 copy.103
  44.3 0.1 fusion.37
  44.4 0.6 reshape.184.outer
  45.1 0.1 copy.104
  45.2 0.8 copy.105.column
  46.0 0.6 copy.97
  46.6 0.6 broadcast_in_dim.65.gain_a
  47.2 51.7 %all-gather.4.cloned.1.call-done.all_ka.all_va.all_kb.all_vb = bf16[1024,2560]{1,0:T(8,128)(2,1)} async-done(((bf16[128,2560]{1,0:T(8,128)(2,1)}), bf16[1024,2560]{1,0:T(8,128)(2,1)}) %all-gather.4.cloned.1.call-update) | async-done | bytes 5242896 | tf_op jit(solution)/shard_map/all_gather | solution.py:76
  98.9 0.7 broadcast_in_dim.64.peak
  99.6 7.9 %shard_map.181 = (bf16[128,1024]{1,0:T(8,128)(2,1)}, bf16[128,512]{1,0:T(8,128)(2,1)}) custom-call(bf16[128,512]{1,0:T(8,128)(2,1)} %qa.1, bf16[128,512]{1,0:T(8,128)(2,1)} %ka.1, bf16[128,1024]{1,0:T(8,128)(2,1)} %va.1, bf16[128,512]{1,0:T(8,128)(2,1)} %qb.1, bf16[128,512]{1,0:T(8,128)(2,1)} %kb.1, bf16[128,512]{1,0:T(8,128)(2,1)} %vb.1, ...), custom_call_target="tpu_custom_call" | custom-call | flops 1610612736 | bytes 5242880 | tf_op jit(solution)/shard_map/pallas_call | solution.py:118
  107.5 3.0 %fusion.58 = f32[128,2048]{1,0:T(8,128)S(1)} fusion(bf16[128,1024]{1,0:T(8,128)(2,1)} %get-tuple-element.7, bf16[1024,2048]{1,0:T(8,128)(2,1)} %param.29), kind=kOutput, calls=%fused_computation.92 | convolution fusion | flops 536870912 | bytes 5505024 | tf_op jit(solution)/shard_map/ec,se->cs/dot_general | solution.py:181
  110.6 1.3 fusion.13
  111.9 0.0 all-gather.6.cloned.1.call-start
  112.0 0.1 copy.106
  112.1 0.1 eq.60
  112.2 0.1 eq.56
  112.4 0.1 copy.96
  112.5 0.6 reduce-window.6
  113.1 0.2 slice_reduce_fusion
  113.4 0.1 fusion.47
  113.5 0.1 reduce_sum.41
  113.6 0.1 copy.108
  113.7 18.2 %reduce-scatter.3.cloned.1.call-done = bf16[512,128]{0,1:T(8,128)(2,1)} async-done(((bf16[2048,128]{0,1:T(8,128)(2,1)}), bf16[512,128]{0,1:T(8,128)(2,1)}) %reduce-scatter.3.cloned.1.call-update) | async-done | bytes 131088 | tf_op jit(solution)/shard_map/reduce_scatter | solution.py:182
  131.9 1.0 multiply_reduce_fusion
  133.0 5.8 %psum.7 = f32[128]{0:T(128)S(1)} all-reduce(f32[128]{0:T(128)S(1)} %multiply_reduce_fusion), channel_id=1, replica_groups=mesh['sp'=8,'tp'=4] {'tp'}, use_global_device_ids=true, to_apply=%region_8.9 | all-reduce | flops 128 | bytes 1024 | tf_op jit(solution)/shard_map/psum | solution.py:192
  138.7 1.3 convolution_convert_fusion
  140.0 19.8 %all_to_all.10 = bf16[8,64,512]{2,1,0:T(8,128)(2,1)} all-to-all(bf16[8,64,512]{2,1,0:T(8,128)(2,1)S(1)} %bitcast.102), channel_id=1, replica_groups=mesh['sp'=8,'tp'=4] {'sp'}, dimensions={0} | all-to-all | bytes 1048576 | tf_op jit(solution)/shard_map/all_to_all | solution.py:217
  159.9 0.0 reduce-scatter.5.cloned.1.call-start
  159.9 20.8 %all-gather.6.cloned.1.call-done = bf16[8,64,2048]{2,1,0:T(8,128)(2,1)} async-done(((bf16[8,64,512]{2,1,0:T(8,128)(2,1)}), bf16[8,64,2048]{2,1,0:T(8,128)(2,1)}) %all-gather.6.cloned.1.call-update) | async-done | bytes 2097168 | tf_op jit(solution)/shard_map/all_gather | solution.py:218
  180.7 6.5 %fusion.4 = f32[512,1024]{1,0:T(8,128)} fusion(bf16[512,2048]{1,0:T(8,128)(2,1)} %bitcast.114, bf16[1,2048,1024]{2,1,0:T(8,128)(2,1)} %param.35), kind=kOutput, calls=%fused_computation.4 | convolution fusion | flops 2147483648 | bytes 8388608 | tf_op jit(solution)/shard_map/dot_general | solution.py:222
  187.2 10.5 %fusion.9 = bf16[2048,512]{0,1:T(8,128)(2,1)} fusion(bf16[1,1024,2048]{2,1,0:T(8,128)(2,1)} %param.37, f32[512,1024]{1,0:T(8,128)} %fusion.4, bf16[512,2048]{1,0:T(8,128)(2,1)} %bitcast.115, bf16[1,2048,1024]{2,1,0:T(8,128)(2,1)} %param.36), kind=kOutput, calls=%fused_computation.7 | convolution fusion | flops 4299161600 | bytes 14680064 | tf_op jit(solution)/shard_map/rf,fc->cr/dot_general | solution.py:233
  197.7 31.3 %reduce-scatter.5.cloned.1.call-done = bf16[512,512]{0,1:T(8,128)(2,1)} async-done(((bf16[2048,512]{0,1:T(8,128)(2,1)}), bf16[512,512]{0,1:T(8,128)(2,1)}) %reduce-scatter.5.cloned.1.call-update) | async-done | bytes 524304 | tf_op jit(solution)/shard_map/reduce_scatter | solution.py:232
  229.1 5.5 %all-to-all-start.1 = ((bf16[512,8,64]{0,2,1:T(8,128)(2,1)}), bf16[512,8,64]{0,2,1:T(8,128)(2,1)S(1)}, u32[]{:S(2)}, u32[]{:S(2)}) async-start(bf16[512,8,64]{0,2,1:T(8,128)(2,1)} %bitcast.105), calls=%async_computation.3 | async-start | bytes 1048576 | tf_op jit(solution)/shard_map/all_to_all | solution.py:241
  234.6 14.3 %all-to-all-done.1 = bf16[512,8,64]{0,2,1:T(8,128)(2,1)S(1)} async-done(((bf16[512,8,64]{0,2,1:T(8,128)(2,1)}), bf16[512,8,64]{0,2,1:T(8,128)(2,1)S(1)}, u32[]{:S(2)}, u32[]{:S(2)}) %all-to-all-start.1) | async-done | bytes 524320 | tf_op jit(solution)/shard_map/all_to_all | solution.py:241
  248.9 0.3 fusion.17
  249.2 0.3 fusion.18
  249.5 0.8 copy.111
  (43 shorter events, 0.3 us)
Async XLA Ops:
  6.5 104.0 %copy-start = (bf16[512,2048]{1,0:T(8,128)(2,1)S(1)}, bf16[512,2048]{1,0:T(8,128)(2,1)}, u32[]{:S(2)}) copy-start(bf16[512,2048]{1,0:T(8,128)(2,1)} %param.30) | copy-start | bytes 6291460
  6.5 3.5 %copy-start.4 = (f32[2,2,4,128]{3,2,1,0:T(4,128)S(1)}, f32[2,2,4,128]{3,2,1,0:T(4,128)}, u32[]{:S(2)}) copy-start(f32[2,2,4,128]{3,2,1,0:T(4,128)} %param.25) | copy-start | bytes 24580
  6.5 40.1 %copy-start.6 = (f32[4,256]{1,0:T(4,128)S(1)}, f32[4,256]{1,0:T(4,128)}, u32[]{:S(2)}) copy-start(f32[4,256]{1,0:T(4,128)} %param.27) | copy-start | bytes 12292
  6.5 92.4 %all-gather.4.cloned.1.call-start = ((), (), s32[]{:S(2)}) async-start(), calls=%async_computation.4 | async-start | bytes 5898240 | tf_op jit(solution)/shard_map/all_gather | solution.py:76
  8.8 123.2 %reduce-scatter.3.cloned.1.call-start = ((), (), s32[]{:S(2)}) async-start(), calls=%async_computation.5 | async-start | bytes 655360 | tf_op jit(solution)/shard_map/reduce_scatter | solution.py:182
  107.5 3.1 %copy-start.3 = (bf16[128,512]{1,0:T(8,128)(2,1)S(1)}, bf16[128,512]{1,0:T(8,128)(2,1)}, u32[]{:S(2)}) copy-start(bf16[128,512]{1,0:T(8,128)(2,1)} %get-tuple-element.8) | copy-start | bytes 393220
  110.6 1.4 copy-start.5
  110.6 1.8 copy-start.2
  110.6 28.1 %copy-start.7 = (f32[512]{0:T(512)S(1)}, f32[512]{0:T(512)}, u32[]{:S(2)}) copy-start(f32[512]{0:T(512)} %param.32) | copy-start | bytes 6148
  111.9 68.8 %all-gather.6.cloned.1.call-start = ((), (), s32[]{:S(2)}) async-start(), calls=%async_computation.6 | async-start | bytes 2621440 | tf_op jit(solution)/shard_map/all_gather | solution.py:218
  159.9 69.2 %reduce-scatter.5.cloned.1.call-start = ((), (), s32[]{:S(2)}) async-start(), calls=%async_computation.7 | async-start | bytes 2621440 | tf_op jit(solution)/shard_map/reduce_scatter | solution.py:232
  197.7 36.9 %copy-start.8 = (f32[128,2]{0,1:T(2,128)S(1)}, f32[128,2]{0,1:T(2,128)}, u32[]{:S(2)}) copy-start(f32[128,2]{0,1:T(2,128)} %param.34) | copy-start | bytes 3076
  197.7 51.2 %copy-start.1 = (bf16[512,128]{0,1:T(8,128)(2,1)S(1)}, bf16[512,128]{0,1:T(8,128)(2,1)}, u32[]{:S(2)}) copy-start(bf16[512,128]{0,1:T(8,128)(2,1)} %reduce-scatter.3.cloned.1.call-done) | copy-start | bytes 393220
  229.1 19.8 %all-to-all-start.1 = ((bf16[512,8,64]{0,2,1:T(8,128)(2,1)}), bf16[512,8,64]{0,2,1:T(8,128)(2,1)S(1)}, u32[]{:S(2)}, u32[]{:S(2)}) async-start(bf16[512,8,64]{0,2,1:T(8,128)(2,1)} %bitcast.105), calls=%async_computation.3 | async-start | bytes 1048576 | tf_op jit(solution)/shard_map/all_to_all | solution.py:241
Sparse Core Ops, SparseCore 0:
  9.5 89.3 all-gather.3
  112.0 19.8 reduce-scatter.2
  160.0 20.6 all-gather.5
  197.9 31.1 reduce-scatter.4

commit v2 on v1

--- a/solution.py
+++ b/solution.py
@@ -1,3 +1,5 @@
+import functools
+
 import jax
 import jax.numpy as jnp
 from jax import lax
@@ -15,7 +17,156 @@
     )
 
 
-def one_head(query, key, value, keys, values, inner_row, outer_row, column, peak, gain):
+MESH = pl.DeviceIdType.MESH
+
+
+def greet(peers):
+    barrier = pltpu.get_barrier_semaphore()
+    for peer in peers:
+        pl.semaphore_signal(barrier, inc=1, device_id=peer, device_id_type=MESH)
+    pl.semaphore_wait(barrier, len(peers))
+
+
+def exchange_kernel(count, arrays, *refs):
+    given, taken = refs[:arrays], refs[arrays : 2 * arrays]
+    sent, landed, kept = refs[2 * arrays :]
+    mine = lax.axis_index("sp")
+    peers = [lax.rem(mine + step, count) for step in range(1, count)]
+    greet([{"sp": peer} for peer in peers])
+    copies = []
+    for step, peer in enumerate(peers):
+        for a in range(arrays):
+            copy = pltpu.make_async_remote_copy(
+                src_ref=given[a].at[peer],
+                dst_ref=taken[a].at[mine],
+                send_sem=sent.at[a, step],
+                recv_sem=landed.at[a, step],
+                device_id={"sp": peer},
+                device_id_type=MESH,
+            )
+            copy.start()
+            copies.append(copy)
+    for a in range(arrays):
+        copy = pltpu.make_async_copy(given[a].at[mine], taken[a].at[mine], kept.at[a])
+        copy.start()
+        copies.append(copy)
+    for copy in copies:
+        copy.wait()
+
+
+def exchange(arrays, number):
+    count = arrays[0].shape[0]
+    spec = pl.BlockSpec(memory_space=pltpu.VMEM)
+    return pl.pallas_call(
+        functools.partial(exchange_kernel, count, len(arrays)),
+        out_shape=[jax.ShapeDtypeStruct(a.shape, a.dtype) for a in arrays],
+        in_specs=[spec] * len(arrays),
+        out_specs=[spec] * len(arrays),
+        scratch_shapes=[
+            pltpu.SemaphoreType.DMA((len(arrays), count - 1)),
+            pltpu.SemaphoreType.DMA((len(arrays), count - 1)),
+            pltpu.SemaphoreType.DMA((len(arrays),)),
+        ],
+        compiler_params=pltpu.CompilerParams(collective_id=number, has_side_effects=True),
+    )(*arrays)
+
+
+def dispatch_kernel(count, across, given, taken, sent, landed, kept, y_sent, y_landed, c_sent, c_landed):
+    mine, slot = lax.axis_index("sp"), lax.axis_index("tp")
+    chips = across // 2
+    width = given.shape[-1]
+    twin = slot + 1 - 2 * lax.rem(slot, 2)
+    others = [lax.rem(slot + 2 * step, across) for step in range(1, chips)]
+    behind = [lax.rem(slot + across - 2 * step, across) for step in range(1, chips)]
+    peers = [lax.rem(mine + step, count) for step in range(1, count)]
+    greet([{"sp": peer} for peer in peers] + [{"tp": other} for other in others] + [{"tp": twin}])
+
+    def place(source, owner):
+        return taken.at[source, :, pl.ds(pl.multiple_of(owner * width, width), width)]
+
+    def forward(source, owner, target, send, land):
+        copy = pltpu.make_async_remote_copy(
+            src_ref=place(source, owner),
+            dst_ref=place(source, owner),
+            send_sem=send,
+            recv_sem=land,
+            device_id={"tp": target},
+            device_id_type=MESH,
+        )
+        copy.start()
+        return copy
+
+    own = pltpu.make_async_copy(given.at[mine], place(mine, slot), kept.at[0])
+    own.start()
+    first = []
+    for step, peer in enumerate(peers):
+        copy = pltpu.make_async_remote_copy(
+            src_ref=given.at[peer],
+            dst_ref=place(mine, slot),
+            send_sem=sent.at[step],
+            recv_sem=landed.at[step],
+            device_id={"sp": peer},
+            device_id_type=MESH,
+        )
+        copy.start()
+        first.append(copy)
+    sources = [lax.rem(mine + count - step, count) for step in range(count)]
+    along, last = [], []
+
+    def hand_over(step):
+        for turn, owner in enumerate(behind):
+            along[step][turn].wait_recv()
+            last.append(
+                forward(
+                    sources[step], owner, twin, c_sent.at[step, turn + 1], c_landed.at[step, turn + 1]
+                )
+            )
+
+    for step in range(count):
+        if step == 0:
+            own.wait()
+        else:
+            first[step - 1].wait_recv()
+        along.append(
+            [
+                forward(sources[step], slot, other, y_sent.at[step, turn], y_landed.at[step, turn])
+                for turn, other in enumerate(others)
+            ]
+        )
+        last.append(forward(sources[step], slot, twin, c_sent.at[step, 0], c_landed.at[step, 0]))
+        if step > 0:
+            hand_over(step - 1)
+    hand_over(count - 1)
+    for copy in first:
+        copy.wait_send()
+    for copies in along:
+        for copy in copies:
+            copy.wait_send()
+    for copy in last:
+        copy.wait()
+
+
+def dispatch_rows(buffer, number):
+    count, rows, width = buffer.shape
+    across = lax.axis_size("tp")
+    chips = across // 2
+    spec = pl.BlockSpec(memory_space=pltpu.VMEM)
+    dma = pltpu.SemaphoreType.DMA
+    return pl.pallas_call(
+        functools.partial(dispatch_kernel, count, across),
+        out_shape=jax.ShapeDtypeStruct((count, rows, width * across), buffer.dtype),
+        in_specs=[spec],
+        out_specs=spec,
+        scratch_shapes=[
+            dma((count - 1,)), dma((count - 1,)), dma((1,)),
+            dma((count, chips - 1)), dma((count, chips - 1)),
+            dma((count, chips)), dma((count, chips)),
+        ],
+        compiler_params=pltpu.CompilerParams(collective_id=number, has_side_effects=True),
+    )(buffer)
+
+
+def one_head(query, key, value, keys, values, inner_row, outer_row, column, peak, gain, share):
     length, width_k = query.shape
     scale = width_k ** (-0.5)
     rows = lax.broadcasted_iota(jnp.int32, (length, length), 0)
@@ -43,7 +194,7 @@
         denom = carried * far_sums[r] + jnp.sum(scores, axis=1, keepdims=True)
         out = numer / jnp.maximum(jnp.abs(denom), jnp.exp(-top))
         both = out if both is None else both + out
-    mean = jnp.mean(both * both, axis=1, keepdims=True)
+    mean = jnp.sum(both * both, axis=1, keepdims=True) * share
     return (both * lax.rsqrt(mean + EPSILON) * gain).astype(jnp.bfloat16)
 
 
@@ -63,6 +214,7 @@
             [column[0, :, 2 * r + g : 2 * r + g + 1] for r in range(2)],
             [peak[0, 2 * r + g : 2 * r + g + 1, 0:1] for r in range(2)],
             gain[0],
+            1.0 / gain.shape[-1],
         )
 
 
@@ -150,6 +302,132 @@
         query_a, key_a, value_a, query_b, key_b, value_b,
         gathered, gathered, gathered, gathered,
         inner, outer, column, peak, gain_a[:, None, :], gain_b[:, None, :],
+    )
+
+
+def unit_kernel(q, k, v, every_k, every_v, inner, outer, column, peak, gain, share, heads):
+    heads[0] = one_head(
+        q[0], k[0], v[0], every_k[...].reshape(-1, every_k.shape[-1]),
+        every_v[...].reshape(-1, every_v.shape[-1]),
+        [inner[0, r : r + 1, :] for r in range(2)],
+        [outer[0, r : r + 1, :] for r in range(2)],
+        [column[0, :, r : r + 1] for r in range(2)],
+        [peak[0, r : r + 1, 0:1] for r in range(2)],
+        gain[...],
+        share[0:1, 0:1],
+    )
+
+
+def mix_units(query_a, key_a, value_a, query_b, key_b, value_b, in_gate, forget_gate, gain_a, gain_b):
+    heads = gain_a.shape[0]
+    length = query_a.shape[0]
+    width_k = query_a.shape[1] // heads
+    width_a, width_b = gain_a.shape[1], gain_b.shape[1]
+    count, mine = lax.axis_size("sp"), lax.axis_index("sp")
+
+    def widen(array, axis):
+        pads = [(0, 0)] * array.ndim
+        pads[axis] = (0, width_a - width_b)
+        return jnp.pad(array, pads)
+
+    def cut(values, queries, keys, width):
+        parts = []
+        for h in range(heads):
+            value = values[:, h * width : (h + 1) * width]
+            parts.append(
+                jnp.concatenate(
+                    [
+                        value if width == width_a else widen(value, 1),
+                        queries[:, h * width_k : (h + 1) * width_k],
+                        keys[:, h * width_k : (h + 1) * width_k],
+                    ],
+                    axis=1,
+                )
+            )
+        return parts
+
+    packed = jnp.stack(
+        cut(value_a, query_a, key_a, width_a) + cut(value_b, query_b, key_b, width_b)
+    )
+    log_decay = jax.nn.log_sigmoid(forget_gate)
+    gates = jnp.stack([in_gate, log_decay], axis=2)
+    gates = gates.transpose(1, 3, 0, 2, 4).reshape(count, 4, length)
+    gates = jnp.concatenate([gates, jnp.zeros_like(gates)], axis=1)
+    rows, gates = exchange([packed, gates], 0)
+    in_rows, decay = gates[:, 0:4:2], gates[:, 1:4:2]
+    ones = jnp.ones((length, length), jnp.float32)
+    exact = lax.Precision.HIGHEST
+    run = jnp.stack(
+        [
+            jnp.dot(decay[:, 0], jnp.triu(ones), precision=exact),
+            jnp.dot(decay[:, 1], jnp.tril(ones), precision=exact),
+        ],
+        axis=1,
+    )
+    whole = jnp.sum(decay, axis=-1)
+    tails = in_rows + whole[..., None] - run
+    place = jnp.arange(count)
+    reader, source, middle = place[:, None, None], place[None, :, None], place[None, None, :]
+    between = jnp.stack(
+        [
+            (middle > source) & (middle < reader),
+            (middle < source) & (middle > reader),
+        ],
+        axis=1,
+    ).astype(jnp.float32)
+    gap = jnp.sum(between * whole.T[None, :, None, :], axis=-1)
+    seen = jnp.stack([source < reader, source > reader], axis=1)
+    logs = jnp.where(seen, tails.transpose(1, 0, 2)[None] + gap[..., None], NOTHING)
+    peak = jnp.max(logs, axis=(2, 3))
+    outer = jnp.where(seen, jnp.exp(logs - peak[:, :, None, None]), 0.0)
+    outer = outer.reshape(count, 2, count * length)
+    peak = jnp.broadcast_to(peak[:, :, None], (count, 2, 128))
+    inner = in_rows - run
+    column = run.transpose(0, 2, 1)
+    gains = jnp.concatenate([gain_a, widen(gain_b, 1)], axis=0)
+    gain = lax.dynamic_slice_in_dim(gains, mine, 1, 0)
+    share = jnp.full((1, 128), jnp.where(mine < heads, 1.0 / width_a, 1.0 / width_b), jnp.float32)
+    first_q, first_k = width_a // width_k, width_a // width_k + 1
+
+    def block(width, first):
+        return pl.BlockSpec((1, length, width), lambda t: (t, 0, first))
+
+    def every(width, first):
+        return pl.BlockSpec((count, length, width), lambda t: (0, 0, first))
+
+    def by_block(*shape):
+        return pl.BlockSpec((1,) + shape, lambda t: (t, 0, 0))
+
+    def fixed(*shape):
+        return pl.BlockSpec(shape, lambda t: (0, 0))
+
+    out = pl.pallas_call(
+        unit_kernel,
+        grid=(count,),
+        in_specs=[
+            block(width_k, first_q),
+            block(width_k, first_k),
+            block(width_a, 0),
+            every(width_k, first_k),
+            every(width_a, 0),
+            by_block(2, length),
+            by_block(2, count * length),
+            by_block(length, 2),
+            by_block(2, 128),
+            fixed(1, width_a),
+            fixed(1, 128),
+        ],
+        out_specs=block(width_a, 0),
+        out_shape=jax.ShapeDtypeStruct((count, length, width_a), jnp.bfloat16),
+    )(rows, rows, rows, rows, rows, inner, outer, column, peak, gain, share)
+    (units,) = exchange([out], 1)
+
+    def lay(parts):
+        return jnp.concatenate(parts, axis=1)
+
+    return (
+        lay([units[h] for h in range(heads)]),
+        lay([units[heads + h][:, :width_b] for h in range(heads)]),
     )
 
 
@@ -174,7 +452,8 @@
     expert_up,
     expert_down,
 ):
-    heads_a, heads_b = mix_heads(
+    whole_heads = 2 * head_gain_a.shape[0] == lax.axis_size("sp")
+    heads_a, heads_b = (mix_units if whole_heads else mix_heads)(
         query_a, key_a, value_a, query_b, key_b, value_b,
         in_gate, forget_gate, head_gain_a, head_gain_b,
     )
@@ -214,8 +493,7 @@
     dispatch = dispatch + selectors[ordering_index]
     buffer = jnp.einsum("ps,ds->pd", dispatch, normed, preferred_element_type=jnp.float32)
     buffer = buffer.astype(jnp.bfloat16).reshape(expert_count, slot_count, -1)
-    arrived = lax.all_to_all(buffer, "sp", split_axis=0, concat_axis=0, tiled=True)
-    piece = lax.all_gather(arrived, "tp", axis=2, tiled=True)
+    piece = dispatch_rows(buffer, 2)
     flat_rows = piece.reshape(-1, piece.shape[-1])
     gate_rows = expert_gate[0]
     up_rows = expert_up[0]
@@ -224,7 +502,7 @@
     hidden = (
         (jax.nn.silu(gate) * upward)
         .astype(jnp.bfloat16)
-        .reshape(arrived.shape[0], arrived.shape[1], -1)
+        .reshape(expert_count, slot_count, -1)
     )
     sources = hidden.shape[0]
     hidden_rows = hidden.reshape(-1, hidden.shape[-1])

time: 257 us -> 221 us (0.86)
  Pallas kernels: 7.9 us -> 81.6 us
  waiting for transfers between devices: 136 us -> 70 us
  blocking collectives: 59 us -> 5.75 us
  local copies, waits for them, and re-layouts: 5.55 us -> 12.4 us
    pallas_call x1 -> x4, Pallas kernels: 7.9 us -> 81.6 us  [the longest x2 46.2 us: exchange(): pl.pallas_call(functools.partial(exchange_kernel, count, len(arrays)), ou...]
    all_gather x2 -> x0, waiting for transfers between devices: 72.5 us -> none  [the longest x1 51.7 us: mix_heads(): gathered = lax.all_gather(packed, 'sp', axis=0, tiled=True)]
    all_gather x1 -> x0, blocking collectives: 33.4 us -> none  [mix_heads(): lax.all_gather(jnp.stack([tails, jnp.broadcast_to(whole, tails.shape)]),...]
    all_to_all x1 -> x0, blocking collectives: 19.8 us -> none  [local(): lax.all_to_all(buffer, 'sp', split_axis=0, concat_axis=0, tiled=True)]
    slice x3 -> x12, local copies, waits for them, and re-layouts: 0.22 us -> 5.5 us  [the longest x2 1.91 us: cut(): value = values[:, h * width:(h + 1) * width]]
    reduce_scatter x1, waiting for transfers between devices: 18.2 us -> 23 us  [local(): lax.psum_scatter((first_term + jnp.einsum('ec,se->cs', out_weight_b, head...]
  transfers between devices with their start and end apart: 5 -> 3, of which waited for: 5 -> 3; matrix products, arithmetic and copies ran while one was open for 3% -> 1% of each run, Pallas kernels for 0% -> 0%
where the time goes in v2:
time: 221 us; the launch traced here: 220 us
  Pallas kernels  81.6 us (37%)
  waiting for transfers between devices  70 us (32%)
  matrix products  24.2 us (11%)
  between operations  13.8 us (6%)
  local copies, waits for them, and re-layouts  12.4 us (6%)
  other arithmetic  6.56 us (3%)
  blocking collectives  5.75 us (3%)
  starting transfers between devices  5.55 us (3%)
    pallas_call x2, Pallas kernels, exchange(): pl.pallas_call(functools.partial(exchange_kernel, count, len(arrays)), ou...  46.2 us
    reduce_scatter x1, waiting for transfers between devices, local(): lax.psum_scatter(jnp.einsum('rf,fc->cr', hidden_rows, columns, preferred_...  32.6 us
    pallas_call x1, Pallas kernels, dispatch_rows(): pl.pallas_call(functools.partial(dispatch_kernel, count, across), out_sha...  26.6 us
    reduce_scatter x1, waiting for transfers between devices, local(): lax.psum_scatter((first_term + jnp.einsum('ec,se->cs', out_weight_b, head...  23 us
    all_to_all x1, waiting for transfers between devices, local(): lax.all_to_all(outgoing, 'sp', split_axis=1, concat_axis=1, tiled=True)  14.3 us
    dot_general x1, matrix products, local(): jnp.einsum('rf,fc->cr', hidden_rows, columns, preferred_element_type=jnp....  10.5 us
    pallas_call x1, Pallas kernels, mix_units(): pl.pallas_call(unit_kernel, grid=(count,), in_specs=[block(width_k, first...  8.8 us
    dot_general x1, matrix products, local(): gate = jnp.dot(flat_rows, gate_rows, preferred_element_type=jnp.float32)  6.49 us
  transfers between devices with their start and end apart: 3, of which 3 were waited for; matrix products, arithmetic and copies ran while one was open for 1% of the time, Pallas kernels for 0%

profile of v2, /device:TPU:0, one launch (start us, length us, event | category | flops | bytes accessed | tf_op | source)
XLA Modules:
  0.0 219.8 jit_solution(2927015832219866738)
XLA Ops:
  6.5 1.1 fusion.90
  7.6 0.8 fusion.93
  8.5 0.9 slice_select_fusion
  9.3 0.7 fusion.77
  10.0 0.7 maximum_bitcast_fusion.5
  10.7 0.9 fusion.94
  11.7 0.9 fusion.91
  12.6 0.6 concatenate.44.refs_1_
  13.4 1.0 copy-done.1
  14.4 25.9 %shard_map.181 = (bf16[8,128,512]{2,1,0:T(8,128)(2,1)}, f32[8,8,128]{2,1,0:T(8,128)}) custom-call(bf16[8,128,512]{2,1,0:T(8,128)(2,1)} %copy-done.1, f32[8,8,128]{2,1,0:T(8,128)} %concatenate.44.refs_1_), custom_call_target="tpu_custom_call" | custom-call | tf_op jit(solution)/shard_map/pallas_call | solution.py:60
  40.3 0.8 slice.164
  41.1 0.8 slice.163
  41.9 0.1 convolution_bitcast_fusion
  42.1 0.2 convolution_bitcast_fusion.1
  42.3 1.1 copy.125
  43.4 0.6 fusion.88
  44.1 0.1 select_reduce_fusion.1
  44.3 0.2 select_reduce_fusion
  44.8 0.6 fusion.80.gain
  45.4 0.8 copy_select_fusion.1.outer
  46.2 0.7 broadcast_in_dim.63.peak
  46.8 0.5 broadcast_in_dim.64.share
  47.3 8.8 %shard_map.182.refs_0_ = bf16[8,128,256]{2,1,0:T(8,128)(2,1)} custom-call(bf16[8,128,512]{2,1,0:T(8,128)(2,1)} %get-tuple-element.7.q.k.v.every_k.every_v, bf16[8,128,512]{2,1,0:T(8,128)(2,1)} %get-tuple-element.7.q.k.v.every_k.every_v, bf16[8,128,512]{2,1,0:T(8,128)(2,1)} %get-tuple-element.7.q.k.v.every_k.every_v, ...), custom_call_target="tpu_custom_call" | custom-call | tf_op jit(solution)/shard_map/pallas_call | solution.py:404
  56.1 20.4 %shard_map.183 = bf16[8,128,256]{2,1,0:T(8,128)(2,1)} custom-call(bf16[8,128,256]{2,1,0:T(8,128)(2,1)} %shard_map.182.refs_0_), custom_call_target="tpu_custom_call" | custom-call | tf_op jit(solution)/shard_map/pallas_call | solution.py:60
  76.5 1.1 slice_bitcast_fusion.3
  77.6 2.9 %fusion.24 = f32[128,2048]{1,0:T(8,128)S(1)} fusion(bf16[1024,2048]{1,0:T(8,128)(2,1)} %param.29, bf16[128,256]{1,0:T(8,128)(2,1)S(1)} %get-tuple-element.13, bf16[128,256]{1,0:T(8,128)(2,1)S(1)} %get-tuple-element.14, bf16[128,256]{1,0:T(8,128)(2,1)S(1)} %get-tuple-element.15, bf16[128,256]{1,0:T(8,128)(2,1)S(1)} %get-tuple-element.16), kind=kOutput, calls=%fused_computation.24 | convolution fusion | flops 537919488 | bytes 5505024 | tf_op jit(solution)/shard_map/ec,se->cs/dot_general | solution.py:460
  80.6 1.3 fusion.13
  82.0 0.1 copy.127
  82.1 0.1 eq.60
  82.2 0.1 eq.56
  82.4 0.1 copy.114
  82.5 0.6 reduce-window.6
  83.1 0.2 slice_reduce_fusion
  83.4 0.1 fusion.78
  83.5 0.1 reduce_sum.41
  83.7 23.0 %reduce-scatter.3.cloned.1.call-done = bf16[512,128]{0,1:T(8,128)(2,1)} async-done(((bf16[2048,128]{0,1:T(8,128)(2,1)}), bf16[512,128]{0,1:T(8,128)(2,1)}) %reduce-scatter.3.cloned.1.call-update) | async-done | bytes 131088 | tf_op jit(solution)/shard_map/reduce_scatter | solution.py:461
  106.7 1.0 multiply_reduce_fusion
  107.7 5.8 %psum.7 = f32[128]{0:T(128)S(1)} all-reduce(f32[128]{0:T(128)S(1)} %multiply_reduce_fusion), channel_id=1, replica_groups=mesh['sp'=8,'tp'=4] {'tp'}, use_global_device_ids=true, to_apply=%region_8.9 | all-reduce | flops 128 | bytes 1024 | tf_op jit(solution)/shard_map/psum | solution.py:471
  113.5 2.1 convolution_convert_fusion
  115.6 26.6 %shard_map.184 = bf16[8,64,2048]{2,1,0:T(8,128)(2,1)} custom-call(bf16[8,64,512]{2,1,0:T(8,128)(2,1)} %bitcast.128), custom_call_target="tpu_custom_call" | custom-call | tf_op jit(solution)/shard_map/pallas_call | solution.py:155
  142.1 6.5 %fusion.4 = f32[512,1024]{1,0:T(8,128)} fusion(bf16[512,2048]{1,0:T(8,128)(2,1)} %bitcast.126, bf16[1,2048,1024]{2,1,0:T(8,128)(2,1)} %param.35), kind=kOutput, calls=%fused_computation.4 | convolution fusion | flops 2147483648 | bytes 8388608 | tf_op jit(solution)/shard_map/dot_general | solution.py:500
  148.6 10.5 %fusion.9 = bf16[2048,512]{0,1:T(8,128)(2,1)} fusion(bf16[1,1024,2048]{2,1,0:T(8,128)(2,1)} %param.37, f32[512,1024]{1,0:T(8,128)} %fusion.4, bf16[512,2048]{1,0:T(8,128)(2,1)} %bitcast.127, bf16[1,2048,1024]{2,1,0:T(8,128)(2,1)} %param.36), kind=kOutput, calls=%fused_computation.7 | convolution fusion | flops 4299161600 | bytes 14680064 | tf_op jit(solution)/shard_map/rf,fc->cr/dot_general | solution.py:511
  159.2 32.6 %reduce-scatter.5.cloned.1.call-done = bf16[512,512]{0,1:T(8,128)(2,1)} async-done(((bf16[2048,512]{0,1:T(8,128)(2,1)}), bf16[512,512]{0,1:T(8,128)(2,1)}) %reduce-scatter.5.cloned.1.call-update) | async-done | bytes 524304 | tf_op jit(solution)/shard_map/reduce_scatter | solution.py:510
  191.8 5.5 %all-to-all-start = ((bf16[512,8,64]{0,2,1:T(8,128)(2,1)}), bf16[512,8,64]{0,2,1:T(8,128)(2,1)S(1)}, u32[]{:S(2)}, u32[]{:S(2)}) async-start(bf16[512,8,64]{0,2,1:T(8,128)(2,1)} %bitcast.130), calls=%async_computation.2 | async-start | bytes 1048576 | tf_op jit(solution)/shard_map/all_to_all | solution.py:519
  197.4 14.3 %all-to-all-done = bf16[512,8,64]{0,2,1:T(8,128)(2,1)S(1)} async-done(((bf16[512,8,64]{0,2,1:T(8,128)(2,1)}), bf16[512,8,64]{0,2,1:T(8,128)(2,1)S(1)}, u32[]{:S(2)}, u32[]{:S(2)}) %all-to-all-start) | async-done | bytes 524320 | tf_op jit(solution)/shard_map/all_to_all | solution.py:519
  211.7 0.3 fusion.17
  212.0 0.3 fusion.18
  212.2 0.8 copy.132
  (58 shorter events, 0.9 us)
Async XLA Ops:
  6.5 74.0 %copy-start = (bf16[512,2048]{1,0:T(8,128)(2,1)S(1)}, bf16[512,2048]{1,0:T(8,128)(2,1)}, u32[]{:S(2)}) copy-start(bf16[512,2048]{1,0:T(8,128)(2,1)} %param.30) | copy-start | bytes 6291460
  6.5 100.2 %reduce-scatter.3.cloned.1.call-start = ((), (), s32[]{:S(2)}) async-start(), calls=%async_computation.3 | async-start | bytes 655360 | tf_op jit(solution)/shard_map/reduce_scatter | solution.py:461
  13.2 31.6 %copy-start.5 = (f32[4,256]{1,0:T(4,128)S(1)}, f32[4,256]{1,0:T(4,128)}, u32[]{:S(2)}) copy-start(f32[4,256]{1,0:T(4,128)} %param.27) | copy-start | bytes 12292
  13.2 31.6 %copy-start.7 = (f32[4,128]{1,0:T(4,128)S(1)}, f32[4,128]{1,0:T(4,128)}, u32[]{:S(2)}) copy-start(f32[4,128]{1,0:T(4,128)} %param.28) | copy-start | bytes 6148
  13.4 1.0 copy-start.1
  80.6 1.4 copy-start.4
  80.6 1.8 copy-start.3
  80.6 32.9 %copy-start.6 = (f32[512]{0:T(512)S(1)}, f32[512]{0:T(512)}, u32[]{:S(2)}) copy-start(f32[512]{0:T(512)} %param.32) | copy-start | bytes 6148
  81.9 109.9 %reduce-scatter.5.cloned.1.call-start = ((), (), s32[]{:S(2)}) async-start(), calls=%async_computation.4 | async-start | bytes 2621440 | tf_op jit(solution)/shard_map/reduce_scatter | solution.py:510
  159.2 38.2 %copy-start.8 = (f32[128,2]{0,1:T(2,128)S(1)}, f32[128,2]{0,1:T(2,128)}, u32[]{:S(2)}) copy-start(f32[128,2]{0,1:T(2,128)} %param.34) | copy-start | bytes 3076
  159.2 52.5 %copy-start.2 = (bf16[512,128]{0,1:T(8,128)(2,1)S(1)}, bf16[512,128]{0,1:T(8,128)(2,1)}, u32[]{:S(2)}) copy-start(bf16[512,128]{0,1:T(8,128)(2,1)} %reduce-scatter.3.cloned.1.call-done) | copy-start | bytes 393220
  191.8 19.8 %all-to-all-start = ((bf16[512,8,64]{0,2,1:T(8,128)(2,1)}), bf16[512,8,64]{0,2,1:T(8,128)(2,1)S(1)}, u32[]{:S(2)}, u32[]{:S(2)}) async-start(bf16[512,8,64]{0,2,1:T(8,128)(2,1)} %bitcast.130), calls=%async_computation.2 | async-start | bytes 1048576 | tf_op jit(solution)/shard_map/all_to_all | solution.py:519
Sparse Core Ops, SparseCore 0:
  82.0 24.6 reduce-scatter.2
  159.3 32.4 reduce-scatter.4
